TPU v7x, 32 devices: a whole 2x2x4 slice. The times are simulated.
32 devices in a mesh: rep: 4 (over z), fs: 4 (over y, x), tp: 2 (over core).
Axes of the slice: x: 2, y: 2, z: 4, core: 2. Of those that a mesh axis runs over, the one named last changes fastest.
Arguments:
- hidden_in: bfloat16 [2048, 2048], P('rep'), may hold values from -6 to 6
- cotangent: bfloat16 [2048, 2048], P('rep'), may hold values from -3 to 3
- w_up: bfloat16 [2048, 8192], P('rep', ('fs', 'tp')), may hold values from -0.125 to 0.125
- w_down: bfloat16 [8192, 2048], P(('fs', 'tp'), 'rep'), may hold values from -0.0625 to 0.0625
Outputs:
- input_grad: bfloat16 [2048, 2048], P('rep')
- up_grad: float32 [2048, 8192], P('rep', ('fs', 'tp'))
- down_grad: float32 [8192, 2048], P(('fs', 'tp'), 'rep')
All inputs are finite; a program needn't handle non-finite values.
Results may differ from a plain program's by a relative error of at most 0.017.
Values may be sent and summed in bfloat16 or wider, within the bound.
A program may use at most 64 MiB of HBM per device.

v0:
```python
import jax
import jax.numpy as jnp
from jax import lax
from jax.sharding import PartitionSpec as P


def contract_last(left, right):
    return lax.dot_general(
        left, right, (((1,), (1,)), ((), ())), preferred_element_type=jnp.float32
    )


def contract_first(left, right):
    return lax.dot_general(
        left, right, (((0,), (0,)), ((), ())), preferred_element_type=jnp.float32
    )


def on_device(hidden_in, cotangent, w_up, w_down):
    up_full = lax.all_gather(w_up, "rep", axis=0, tiled=True)
    back_grad = contract_last(cotangent, lax.all_gather(w_down, "rep", axis=1, tiled=True))
    preact = jnp.dot(hidden_in, up_full, preferred_element_type=jnp.float32)
    active = jnp.maximum(preact, 0.0)
    hidden = (active * active).astype(jnp.bfloat16)
    slopes = (2.0 * active * back_grad).astype(jnp.bfloat16)
    grad_upper = lax.psum_scatter(
        contract_first(hidden_in, slopes).astype(jnp.bfloat16),
        "rep",
        scatter_dimension=0,
        tiled=True,
    ).astype(jnp.float32)
    lower_rows = lax.psum_scatter(
        contract_first(cotangent, hidden).astype(jnp.bfloat16),
        "rep",
        scatter_dimension=0,
        tiled=True,
    ).astype(jnp.float32)
    down_grad = lower_rows.T
    partial_sum = contract_last(slopes, up_full).astype(jnp.bfloat16)
    input_grad = lax.psum(partial_sum, ("fs", "tp")).astype(jnp.float32).astype(jnp.bfloat16)
    return (input_grad, grad_upper, down_grad)


def solution(mesh):
    return jax.shard_map(
        on_device,
        mesh=mesh,
        in_specs=(P("rep", None), P("rep", None), P("rep", ("fs", "tp")), P(("fs", "tp"), "rep")),
        out_specs=(P("rep", None), P("rep", ("fs", "tp")), P(("fs", "tp"), "rep")),
        check_vma=False,
    )
```

profile of v0, /device:TPU:0, one launch (start us, length us, event | category | flops | bytes accessed | tf_op | source)
XLA Modules:
  0.0 414.7 jit_solution(14841434194789787365)
XLA Ops:
  7.2 0.0 copy-start
  7.2 0.0 all-gather.3.cloned.1.call-start
  7.2 0.7 all-gather.3.cloned.1.call-update
  7.9 0.0 all-gather.5.cloned.1.call-start
  8.0 0.7 all-gather.5.cloned.1.call-update
  8.7 0.0 reduce-scatter.3.cloned.1.call-start
  8.7 84.3 %all-gather.3.cloned.1.call-done = bf16[2048,1024]{1,0:T(8,128)(2,1)} async-done(((bf16[512,1024]{1,0:T(8,128)(2,1)}), bf16[2048,1024]{1,0:T(8,128)(2,1)}) %all-gather.3.cloned.1.call-update) | async-done | bytes 4194320 | tf_op jit(solution)/shard_map/all_gather | solution.py:20
  93.1 0.0 copy-done
  93.1 5.8 %fusion.2 = f32[512,1024]{1,0:T(8,128)} fusion(bf16[512,2048]{1,0:T(8,128)(2,1)S(1)} %copy-done, bf16[2048,1024]{1,0:T(8,128)(2,1)} %all-gather.3.cloned.1.call-done), kind=kOutput, calls=%fused_computation.8 | convolution fusion | flops 2147483648 | bytes 8388608 | tf_op jit(solution)/shard_map/dot_general | solution.py:22
  98.9 75.0 %all-gather.5.cloned.1.call-done = bf16[1024,2048]{1,0:T(8,128)(2,1)} async-done(((bf16[1024,512]{1,0:T(8,128)(2,1)}), bf16[1024,2048]{1,0:T(8,128)(2,1)}) %all-gather.5.cloned.1.call-update) | async-done | bytes 4194320 | tf_op jit(solution)/shard_map/all_gather | solution.py:21
  173.9 5.8 %multiply_convert_fusion.1 = bf16[512,1024]{1,0:T(8,128)(2,1)S(1)} fusion(f32[512,1024]{1,0:T(8,128)} %fusion.2, bf16[512,2048]{1,0:T(8,128)(2,1)} %param.5, bf16[1024,2048]{1,0:T(8,128)(2,1)} %all-gather.5.cloned.1.call-done), kind=kOutput, calls=%fused_computation.5 | convolution fusion | flops 2149580800 | bytes 9437184 | tf_op jit(solution)/shard_map/dot_general | solution.py:8
  179.7 4.4 %convert_bitcast_fusion.1 = bf16[2048,1024]{0,1:T(8,128)(2,1)} fusion(bf16[512,1024]{1,0:T(8,128)(2,1)S(1)} %multiply_convert_fusion.1, bf16[512,2048]{1,0:T(8,128)(2,1)S(1)} %copy-done), kind=kOutput, calls=%fused_computation.1 | convolution fusion | flops 2149580800 | bytes 7340032 | tf_op jit(solution)/shard_map/dot_general | solution.py:14
  184.1 0.0 reduce-scatter.3.cloned.1.call-update
  184.1 0.0 reduce-scatter.5.cloned.1.call-start
  184.2 6.6 %convert_bitcast_fusion = bf16[2048,1024]{0,1:T(8,128)(2,1)} fusion(bf16[512,2048]{1,0:T(8,128)(2,1)} %param.5, f32[512,1024]{1,0:T(8,128)} %fusion.2), kind=kOutput, calls=%fused_computation | convolution fusion | flops 2151153664 | bytes 8388608 | tf_op jit(solution)/shard_map/dot_general | solution.py:14
  190.8 0.0 reduce-scatter.5.cloned.1.call-update
  190.8 0.0 all-reduce.2.cloned.1.call-start
  190.8 5.9 %convolution_convert_fusion = bf16[512,2048]{1,0:T(8,128)(2,1)} fusion(bf16[512,1024]{1,0:T(8,128)(2,1)S(1)} %multiply_convert_fusion.1, bf16[2048,1024]{1,0:T(8,128)(2,1)} %all-gather.3.cloned.1.call-done), kind=kOutput, calls=%fused_computation.2 | convolution fusion | flops 2148532224 | bytes 7340032 | tf_op jit(solution)/shard_map/dot_general | solution.py:8
  196.7 0.0 all-reduce.2.cloned.1.call-update
  196.7 62.8 %reduce-scatter.3.cloned.1.call-done = bf16[512,1024]{0,1:T(8,128)(2,1)} async-done(((bf16[2048,1024]{0,1:T(8,128)(2,1)}), bf16[512,1024]{0,1:T(8,128)(2,1)}) %reduce-scatter.3.cloned.1.call-update) | async-done | bytes 1048592 | tf_op jit(solution)/shard_map/reduce_scatter | solution.py:26
  259.6 2.6 copy.7
  262.1 76.9 %reduce-scatter.5.cloned.1.call-done = bf16[512,1024]{0,1:T(8,128)(2,1)} async-done(((bf16[2048,1024]{0,1:T(8,128)(2,1)}), bf16[512,1024]{0,1:T(8,128)(2,1)}) %reduce-scatter.5.cloned.1.call-update) | async-done | bytes 1048592 | tf_op jit(solution)/shard_map/reduce_scatter | solution.py:32
  339.1 2.8 convert_bitcast_fusion.2
  341.9 63.1 %all-reduce.2.cloned.1.call-done = bf16[512,2048]{1,0:T(8,128)(2,1)} async-done(((bf16[512,2048]{1,0:T(8,128)(2,1)}), bf16[512,2048]{1,0:T(8,128)(2,1)}) %all-reduce.2.cloned.1.call-update) | async-done | bytes 2097168 | tf_op jit(solution)/shard_map/psum | solution.py:40
  405.0 3.2 copy.9
Async XLA Ops:
  7.2 85.9 %copy-start = (bf16[512,2048]{1,0:T(8,128)(2,1)S(1)}, bf16[512,2048]{1,0:T(8,128)(2,1)}, u32[]{:S(2)}) copy-start(bf16[512,2048]{1,0:T(8,128)(2,1)} %param.4) | copy-start | bytes 6291460
  7.2 85.9 %all-gather.3.cloned.1.call-start = ((), (), s32[]{:S(2)}) async-start(), calls=%async_computation.2 | async-start | bytes 5242880 | tf_op jit(solution)/shard_map/all_gather | solution.py:20
  7.9 166.0 %all-gather.5.cloned.1.call-start = ((), (), s32[]{:S(2)}) async-start(), calls=%async_computation.3 | async-start | bytes 5242880 | tf_op jit(solution)/shard_map/all_gather | solution.py:21
  8.7 250.9 %reduce-scatter.3.cloned.1.call-start = ((), (), s32[]{:S(2)}) async-start(), calls=%async_computation.5 | async-start | bytes 5242880 | tf_op jit(solution)/shard_map/reduce_scatter | solution.py:26
  184.1 154.9 %reduce-scatter.5.cloned.1.call-start = ((), (), s32[]{:S(2)}) async-start(), calls=%async_computation.6 | async-start | bytes 5242880 | tf_op jit(solution)/shard_map/reduce_scatter | solution.py:32
  190.8 214.2 %all-reduce.2.cloned.1.call-start = ((), (), s32[]{:S(2)}) async-start(), calls=%async_computation.4 | async-start | bytes 4194304 | tf_op jit(solution)/shard_map/psum | solution.py:40
Sparse Core Ops, SparseCore 0:
  9.6 83.4 all-gather.2
  94.6 79.2 all-gather.4
  184.3 75.2 reduce-scatter.2
  261.7 77.2 reduce-scatter.4
  342.7 62.2 all-reduce.1
where the time goes:
time: 415 us
  waiting for transfers between devices  364 us (88%)
  matrix products  28.5 us (7%)
  between operations  13.8 us (3%)
  local copies, waits for them, and re-layouts  5.73 us (1%)
    all_gather x1, waiting for transfers between devices, on_device(): up_full = lax.all_gather(w_up, 'rep', axis=0, tiled=True)  84.3 us
    reduce_scatter x1, waiting for transfers between devices, on_device(): lax.psum_scatter(contract_first(cotangent, hidden).astype(jnp.bfloat16),...  76.9 us
    all_gather x1, waiting for transfers between devices, on_device(): lax.all_gather(w_down, 'rep', axis=1, tiled=True)  75 us
    psum x1, waiting for transfers between devices, on_device(): lax.psum(partial_sum, ('fs', 'tp')).astype(jnp.float32).astype(jnp.bfloat16)  63.1 us
    reduce_scatter x1, waiting for transfers between devices, on_device(): lax.psum_scatter(contract_first(hidden_in, slopes).astype(jnp.bfloat16),...  62.8 us
    dot_general x2, matrix products, contract_last(): lax.dot_general(left, right, (((1,), (1,)), ((), ())), preferred_element_...  11.7 us
    dot_general x2, matrix products, contract_first(): lax.dot_general(left, right, (((0,), (0,)), ((), ())), preferred_element_...  10.9 us
  transfers between devices with their start and end apart: 5, of which 5 were waited for; matrix products, arithmetic and copies ran while one was open for 6% of the time, Pallas kernels for 0%

commit v1 on v0

--- a/solution.py
+++ b/solution.py
@@ -17,7 +17,12 @@
 
 
 def on_device(hidden_in, cotangent, w_up, w_down):
-    up_full = lax.all_gather(w_up, "rep", axis=0, tiled=True)
+    ring = [w_up]
+    for hop in range(3):
+        ring.append(lax.ppermute(ring[-1], "rep", [(dev, (dev + 1) % 4) for dev in range(4)]))
+    up_full = jnp.roll(
+        jnp.concatenate(ring[::-1], axis=0), (lax.axis_index("rep") + 1) * ring[0].shape[0], axis=0
+    )
     back_grad = contract_last(cotangent, lax.all_gather(w_down, "rep", axis=1, tiled=True))
     preact = jnp.dot(hidden_in, up_full, preferred_element_type=jnp.float32)
     active = jnp.maximum(preact, 0.0)

time: 415 us -> 400 us (0.964)
  waiting for transfers between devices: 364 us -> 311 us
  starting transfers between devices: 0.2 us -> 32.9 us
  local copies, waits for them, and re-layouts: 5.73 us -> 16.9 us
  matrix products: 28.5 us -> 22.2 us
    ppermute x0 -> x3, waiting for transfers between devices: none -> 110 us  [on_device(): lax.ppermute(ring[-1], 'rep', [(dev, (dev + 1) % 4) for dev in range(4)])]
    all_gather x1 -> x0, waiting for transfers between devices: 84.3 us -> none  [on_device(): up_full = lax.all_gather(w_up, 'rep', axis=0, tiled=True)]
    all_gather x1, waiting for transfers between devices: 75 us -> 0.02 us  [on_device(): lax.all_gather(w_down, 'rep', axis=1, tiled=True)]
    ppermute x0 -> x3, starting transfers between devices: none -> 32.6 us  [on_device(): lax.ppermute(ring[-1], 'rep', [(dev, (dev + 1) % 4) for dev in range(4)])]
    reduce_scatter x1, waiting for transfers between devices: 76.9 us -> 60.4 us  [on_device(): lax.psum_scatter(contract_first(cotangent, hidden).astype(jnp.bfloat16),...]
    reduce_scatter x1, waiting for transfers between devices: 62.8 us -> 76.8 us  [on_device(): lax.psum_scatter(contract_first(hidden_in, slopes).astype(jnp.bfloat16),...]
    unnamed x4 -> x25, local copies, waits for them, and re-layouts: 5.73 us -> 16.8 us
  transfers between devices with their start and end apart: 5 -> 7, of which waited for: 5 -> 6; matrix products, arithmetic and copies ran while one was open for 6% -> 8% of each run, Pallas kernels for 0% -> 0%
where the time goes in v1:
time: 400 us
  waiting for transfers between devices  311 us (78%)
  starting transfers between devices  32.9 us (8%)
  matrix products  22.2 us (6%)
  local copies, waits for them, and re-layouts  16.9 us (4%)
  between operations  13.9 us (3%)
    ppermute x3, waiting for transfers between devices, on_device(): lax.ppermute(ring[-1], 'rep', [(dev, (dev + 1) % 4) for dev in range(4)])  110 us
    reduce_scatter x1, waiting for transfers between devices, on_device(): lax.psum_scatter(contract_first(hidden_in, slopes).astype(jnp.bfloat16),...  76.8 us
    psum x1, waiting for transfers between devices, on_device(): lax.psum(partial_sum, ('fs', 'tp')).astype(jnp.float32).astype(jnp.bfloat16)  63.4 us
    reduce_scatter x1, waiting for transfers between devices, on_device(): lax.psum_scatter(contract_first(cotangent, hidden).astype(jnp.bfloat16),...  60.4 us
    ppermute x3, starting transfers between devices, on_device(): lax.ppermute(ring[-1], 'rep', [(dev, (dev + 1) % 4) for dev in range(4)])  32.6 us
    unnamed x25, local copies, waits for them, and re-layouts  16.8 us
    dot_general x2, matrix products, contract_last(): lax.dot_general(left, right, (((1,), (1,)), ((), ())), preferred_element_...  11.3 us
    dot_general x2, matrix products, contract_first(): lax.dot_general(left, right, (((0,), (0,)), ((), ())), preferred_element_...  8.58 us
  transfers between devices with their start and end apart: 7, of which 6 were waited for; matrix products, arithmetic and copies ran while one was open for 8% of the time, Pallas kernels for 0%

profile of v1, /device:TPU:0, one launch (start us, length us, event | category | flops | bytes accessed | tf_op | source)
XLA Modules:
  0.0 399.7 jit_solution(14834524753716908037)
XLA Ops:
  7.2 0.0 copy-start
  7.2 0.0 copy-start.1
  7.2 0.0 all-gather.2.cloned.1.call-start
  7.2 0.7 all-gather.2.cloned.1.call-update
  7.9 0.0 reduce-scatter.5.cloned.1.call-start
  8.0 3.1 collective-permute-start
  11.1 37.6 %collective-permute-done = bf16[512,1024]{1,0:T(8,128)(2,1)S(1)} collective-permute-done((bf16[512,1024]{1,0:T(8,128)(2,1)}, bf16[512,1024]{1,0:T(8,128)(2,1)S(1)}, u32[]{:S(2)}, u32[]{:S(2)}) %collective-permute-start) | collective-permute-done | bytes 1048608 | tf_op jit(solution)/shard_map/ppermute | solution.py:22
  48.7 1.0 copy-done.2
  49.7 14.7 %collective-permute-start.1 = (bf16[512,1024]{1,0:T(8,128)(2,1)S(1)}, bf16[512,1024]{1,0:T(8,128)(2,1)}, u32[]{:S(2)}, u32[]{:S(2)}) collective-permute-start(bf16[512,1024]{1,0:T(8,128)(2,1)S(1)} %collective-permute-done), channel_id=1, source_target_pairs={{0,8},{8,16},{16,24},{24,0},{1,9},{9,17},{17,25},{25,1},{2,10},{10... | collective-permute-start | bytes 3145736 | tf_op jit(solution)/shard_map/ppermute | solution.py:22
  64.4 46.0 %collective-permute-done.1 = bf16[512,1024]{1,0:T(8,128)(2,1)} collective-permute-done((bf16[512,1024]{1,0:T(8,128)(2,1)S(1)}, bf16[512,1024]{1,0:T(8,128)(2,1)}, u32[]{:S(2)}, u32[]{:S(2)}) %collective-permute-start.1) | collective-permute-done | bytes 1048608 | tf_op jit(solution)/shard_map/ppermute | solution.py:22
  110.4 14.7 %collective-permute-start.2 = (bf16[512,1024]{1,0:T(8,128)(2,1)}, bf16[512,1024]{1,0:T(8,128)(2,1)}, u32[]{:S(2)}, u32[]{:S(2)}) collective-permute-start(bf16[512,1024]{1,0:T(8,128)(2,1)} %collective-permute-done.1), channel_id=1, source_target_pairs={{0,8},{8,16},{16,24},{24,0},{1,9},{9,17},{17,25},{25,1},{2,10},{10... | collective-permute-start | bytes 3145736 | tf_op jit(solution)/shard_map/ppermute | solution.py:22
  125.2 25.9 %collective-permute-done.2 = bf16[512,1024]{1,0:T(8,128)(2,1)} collective-permute-done((bf16[512,1024]{1,0:T(8,128)(2,1)}, bf16[512,1024]{1,0:T(8,128)(2,1)}, u32[]{:S(2)}, u32[]{:S(2)}) %collective-permute-start.2) | collective-permute-done | bytes 1048608 | tf_op jit(solution)/shard_map/ppermute | solution.py:22
  151.1 1.3 constant_dynamic-update-slice_fusion.7
  152.4 1.3 constant_dynamic-update-slice_fusion.6
  153.7 0.0 copy-done.3
  153.7 0.1 constant_dynamic-update-slice_fusion.5
  153.8 0.0 copy-done.1
  153.8 0.1 constant_dynamic-update-slice_fusion.4
  153.8 0.0 copy-start.5
  153.9 1.4 constant_dynamic-update-slice_fusion.3
  155.3 1.3 constant_dynamic-update-slice_fusion.2
  156.6 0.1 constant_dynamic-update-slice_fusion.1
  156.7 0.1 constant_dynamic-update-slice_fusion
  156.8 0.0 copy-start.4
  156.8 3.2 copy-done.4
  160.0 0.0 copy-done.5
  160.0 2.4 fusion.2
  162.4 0.0 copy-start.7
  162.4 1.3 copy-done.7
  163.7 0.0 copy-done
  163.7 4.3 %convert_bitcast_fusion = bf16[2048,1024]{0,1:T(8,128)(2,1)} fusion(bf16[512,2048]{1,0:T(8,128)(2,1)S(1)} %copy-done, f32[1024,512]{1,0:T(8,128)S(1)} %fusion.2), kind=kOutput, calls=%fused_computation | convolution fusion | flops 2151153664 | bytes 8388608 | tf_op jit(solution)/shard_map/dot_general | solution.py:14
  168.0 0.0 reduce-scatter.5.cloned.1.call-update
  168.0 0.0 reduce-scatter.3.cloned.1.call-start
  168.0 0.0 all-gather.2.cloned.1.call-done
  168.1 0.0 copy-start.6
  168.1 5.4 %fusion.7 = bf16[512,1024]{0,1:T(8,128)(2,1)S(1)} fusion(f32[1024,512]{1,0:T(8,128)} %copy-done.7, bf16[512,2048]{1,0:T(8,128)(2,1)S(1)} %copy-done, bf16[1024,2048]{1,0:T(8,128)(2,1)} %all-gather.2.cloned.1.call-done), kind=kOutput, calls=%fused_computation.8 | convolution fusion | flops 2149580800 | bytes 9437184 | tf_op jit(solution)/shard_map/dot_general | solution.py:8
  173.5 0.0 copy-done.6
  173.5 4.3 %convert_bitcast_fusion.1 = bf16[2048,1024]{0,1:T(8,128)(2,1)} fusion(bf16[512,1024]{0,1:T(8,128)(2,1)S(1)} %fusion.7, bf16[512,2048]{1,0:T(8,128)(2,1)S(1)} %copy-done.6), kind=kOutput, calls=%fused_computation.1 | convolution fusion | flops 2149580800 | bytes 7340032 | tf_op jit(solution)/shard_map/dot_general | solution.py:14
  177.8 0.0 reduce-scatter.3.cloned.1.call-update
  177.8 0.2 all-reduce.2.cloned.1.call-start
  178.0 5.9 %fusion.4 = bf16[512,2048]{1,0:T(8,128)(2,1)} fusion(bf16[512,1024]{0,1:T(8,128)(2,1)S(1)} %fusion.7, bf16[4096,1024]{1,0:T(8,128)(2,1)} %copy-done.4, s32[]{:T(128)S(6)} %select_n.14), kind=kOutput, calls=%fused_computation.6 | convolution fusion | flops 2148532224 | bytes 7340036 | tf_op jit(solution)/shard_map/dot_general | solution.py:8
  183.9 0.0 all-reduce.2.cloned.1.call-update
  183.9 60.4 %reduce-scatter.5.cloned.1.call-done = bf16[512,1024]{0,1:T(8,128)(2,1)} async-done(((bf16[2048,1024]{0,1:T(8,128)(2,1)}), bf16[512,1024]{0,1:T(8,128)(2,1)}) %reduce-scatter.5.cloned.1.call-update) | async-done | bytes 1048592 | tf_op jit(solution)/shard_map/reduce_scatter | solution.py:37
  244.4 2.8 convert_bitcast_fusion.2
  247.2 76.8 %reduce-scatter.3.cloned.1.call-done = bf16[512,1024]{0,1:T(8,128)(2,1)} async-done(((bf16[2048,1024]{0,1:T(8,128)(2,1)}), bf16[512,1024]{0,1:T(8,128)(2,1)}) %reduce-scatter.3.cloned.1.call-update) | async-done | bytes 1048592 | tf_op jit(solution)/shard_map/reduce_scatter | solution.py:31
  324.0 2.6 copy.8
  326.6 63.4 %all-reduce.2.cloned.1.call-done = bf16[512,2048]{1,0:T(8,128)(2,1)} async-done(((bf16[512,2048]{1,0:T(8,128)(2,1)}), bf16[512,2048]{1,0:T(8,128)(2,1)}) %all-reduce.2.cloned.1.call-update) | async-done | bytes 2097168 | tf_op jit(solution)/shard_map/psum | solution.py:45
  390.0 3.2 copy.18
  (2 shorter events, 0.0 us)
Async XLA Ops:
  7.2 156.5 %copy-start = (bf16[512,2048]{1,0:T(8,128)(2,1)S(1)}, bf16[512,2048]{1,0:T(8,128)(2,1)}, u32[]{:S(2)}) copy-start(bf16[512,2048]{1,0:T(8,128)(2,1)} %param.5) | copy-start | bytes 6291460
  7.2 146.6 %copy-start.1 = (bf16[512,1024]{1,0:T(8,128)(2,1)S(1)}, bf16[512,1024]{1,0:T(8,128)(2,1)}, u32[]{:S(2)}) copy-start(bf16[512,1024]{1,0:T(8,128)(2,1)} %param.6) | copy-start | bytes 3145732
  7.2 160.9 %all-gather.2.cloned.1.call-start = ((), (), s32[]{:S(2)}) async-start(), calls=%async_computation.2 | async-start | bytes 5242880 | tf_op jit(solution)/shard_map/all_gather | solution.py:26
  7.9 236.5 %reduce-scatter.5.cloned.1.call-start = ((), (), s32[]{:S(2)}) async-start(), calls=%async_computation.5 | async-start | bytes 5242880 | tf_op jit(solution)/shard_map/reduce_scatter | solution.py:37
  8.0 40.7 %collective-permute-start = (bf16[512,1024]{1,0:T(8,128)(2,1)}, bf16[512,1024]{1,0:T(8,128)(2,1)S(1)}, u32[]{:S(2)}, u32[]{:S(2)}) collective-permute-start(bf16[512,1024]{1,0:T(8,128)(2,1)} %param.6), channel_id=1, source_target_pairs={{0,8},{8,16},{16,24},{24,0},{1,9},{9,17},{17,25},{25,1},{2,10},{10... | collective-permute-start | bytes 3145736 | tf_op jit(solution)/shard_map/ppermute | solution.py:22
  48.7 1.0 copy-start.2
  49.7 60.8 %collective-permute-start.1 = (bf16[512,1024]{1,0:T(8,128)(2,1)S(1)}, bf16[512,1024]{1,0:T(8,128)(2,1)}, u32[]{:S(2)}, u32[]{:S(2)}) collective-permute-start(bf16[512,1024]{1,0:T(8,128)(2,1)S(1)} %collective-permute-done), channel_id=1, source_target_pairs={{0,8},{8,16},{16,24},{24,0},{1,9},{9,17},{17,25},{25,1},{2,10},{10... | collective-permute-start | bytes 3145736 | tf_op jit(solution)/shard_map/ppermute | solution.py:22
  110.4 40.6 %collective-permute-start.2 = (bf16[512,1024]{1,0:T(8,128)(2,1)}, bf16[512,1024]{1,0:T(8,128)(2,1)}, u32[]{:S(2)}, u32[]{:S(2)}) collective-permute-start(bf16[512,1024]{1,0:T(8,128)(2,1)} %collective-permute-done.1), channel_id=1, source_target_pairs={{0,8},{8,16},{16,24},{24,0},{1,9},{9,17},{17,25},{25,1},{2,10},{10... | collective-permute-start | bytes 3145736 | tf_op jit(solution)/shard_map/ppermute | solution.py:22
  125.2 28.5 %copy-start.3 = (bf16[512,1024]{1,0:T(8,128)(2,1)S(1)}, bf16[512,1024]{1,0:T(8,128)(2,1)}, u32[]{:S(2)}) copy-start(bf16[512,1024]{1,0:T(8,128)(2,1)} %copy-done.2) | copy-start | bytes 3145732
  153.8 6.1 %copy-start.5 = (bf16[512,2048]{1,0:T(8,128)(2,1)S(1)}, bf16[512,2048]{1,0:T(8,128)(2,1)}, u32[]{:S(2)}) copy-start(bf16[512,2048]{1,0:T(8,128)(2,1)} %param.4) | copy-start | bytes 6291460
  156.8 3.2 copy-start.4
  162.4 1.3 copy-start.7
  168.0 156.0 %reduce-scatter.3.cloned.1.call-start = ((), (), s32[]{:S(2)}) async-start(), calls=%async_computation.4 | async-start | bytes 5242880 | tf_op jit(solution)/shard_map/reduce_scatter | solution.py:31
  168.1 5.4 %copy-start.6 = (bf16[512,2048]{1,0:T(8,128)(2,1)S(1)}, bf16[512,2048]{1,0:T(8,128)(2,1)}, u32[]{:S(2)}) copy-start(bf16[512,2048]{1,0:T(8,128)(2,1)} %param.4) | copy-start | bytes 6291460
  177.8 212.2 %all-reduce.2.cloned.1.call-start = ((), (), s32[]{:S(2)}) async-start(), calls=%async_computation.3 | async-start | bytes 4194304 | tf_op jit(solution)/shard_map/psum | solution.py:45
Sparse Core Ops, SparseCore 0:
  9.6 117.3 all-gather.1
  168.1 76.2 reduce-scatter.4
  246.7 77.2 reduce-scatter.2
  327.7 62.2 all-reduce.1
